TPU v7x, 32 devices: a whole 2x2x4 slice. The times are simulated.
32 devices in a mesh: grp: 2 (over y), tp: 4 (over z), dp: 4 (over x, core).
Axes of the slice: x: 2, y: 2, z: 4, core: 2. Of those that a mesh axis runs over, the one named last changes fastest.
Arguments:
- tokens: bfloat16 [128, 8, 2048], P('grp', None, 'dp'), parts along dimension 0, may hold values from -64 to 64
- live_counts: int32 [128], P(('grp', 'dp')), parts along dimension 0, may hold values from 1 to 8, 256 in all
- norm_gain: float32 [2, 2048], P(None, 'dp'), may hold values from 0.1 to 1.9
- w_branch: bfloat16 [2, 2048, 4096], P(None, 'dp', 'tp'), may hold values from -0.125 to 0.125
- w_silu_gate: bfloat16 [2, 2048, 4096], P(None, 'dp', 'tp'), may hold values from -0.125 to 0.125
- conv_weight: float32 [2, 4, 4096], P(None, None, 'tp'), may hold values from -3 to 3
- w_query: bfloat16 [2, 16, 256, 256], P(None, 'tp'), may hold values from -0.375 to 0.375
- w_key: bfloat16 [2, 16, 256, 256], P(None, 'tp'), may hold values from -0.375 to 0.375
- w_value: bfloat16 [2, 16, 256, 256], P(None, 'tp'), may hold values from -0.375 to 0.375
- w_input_gate: bfloat16 [2, 16, 768], P(None, 'tp'), may hold values from -0.21875 to 0.21875
- w_forget_gate: bfloat16 [2, 16, 768], P(None, 'tp'), may hold values from -0.21875 to 0.21875
- bias_input: float32 [2, 16], P(None, 'tp'), may hold values from -2 to 2
- bias_forget: float32 [2, 16], P(None, 'tp'), may hold values from -1 to 5
- out_gain: float32 [2, 16, 256], P(None, 'tp'), may hold values from 0.25 to 4
- skip_gain: float32 [2, 4096], P(None, 'tp'), may hold values from 0.25 to 4
- w_out: bfloat16 [2, 4096, 2048], P(None, 'tp', 'dp'), may hold values from -0.09375 to 0.09375
- conv_state: bfloat16 [2, 128, 3, 4096], P(None, ('grp', 'dp'), None, 'tp'), parts along dimension 1, may hold values from -6 to 6
- memory: float32 [2, 128, 16, 256, 256], P(None, ('grp', 'dp'), 'tp'), parts along dimension 1, may hold values from -0.375 to 0.375
- max_state: float32 [2, 128, 16], P(None, ('grp', 'dp'), 'tp'), parts along dimension 1, may hold values from -4 to 4
Outputs:
- out_tokens: bfloat16 [128, 8, 2048], P('grp', None, 'dp'), parts along dimension 0
- new_conv_state: bfloat16 [2, 128, 3, 4096], P(None, ('grp', 'dp'), None, 'tp'), parts along dimension 1
- new_memory: float32 [2, 128, 16, 256, 256], P(None, ('grp', 'dp'), 'tp'), parts along dimension 1
- new_max: float32 [2, 128, 16], P(None, ('grp', 'dp'), 'tp'), parts along dimension 1
There are 2 independent parts, one for each index of `grp`. A program takes and returns all parts, laid end to end along the dimension named above; an argument that names none is the same for every part. Nothing has to cross between parts.
Inputs may be any that keep to these rules, and one draw needn't show every extreme that they name: `live_counts`: each sequence has at least one live slot; within each part (each independent copy of the problem) the 64 counts sum to 256, so the whole array sums to that times the number of parts; in each part some sequence uses all 8 slots.
All inputs are finite; a program needn't handle non-finite values. No bound on the sum of `live_counts` on one device may be relied on, other than what follows from the above.
Results may differ from a plain program's by a relative error of at most 0.035.
Values may be sent and summed in bfloat16 or wider, within the bound.
A program may use at most 192 MiB of HBM per device.

v0:
```python
import jax
import jax.numpy as jnp
from jax import lax
from jax.sharding import PartitionSpec as P

D = 2048
HEAD_DIM = 256
CONV = 4
LAYERS = 2
epsilon = 1e-06
very_negative = -1e30


def recurrent_cell(
    branch,
    silu_gate,
    live_counts,
    conv_weight,
    w_query,
    w_key,
    w_value,
    w_input_gate,
    w_forget_gate,
    bias_input,
    bias_forget,
    out_gain,
    skip_gain,
    conv_state,
    memory,
    max_state,
):
    local_batch = branch.shape[0]
    steps = branch.shape[1]
    local_width = branch.shape[2]
    local_heads = w_query.shape[0]
    padded = jnp.concatenate([conv_state, branch], axis=1)
    conv_sum = jnp.zeros((local_batch, steps, local_width), jnp.float32)
    for offset in range(CONV):
        conv_sum = (
            conv_sum + padded[:, offset : offset + steps].astype(jnp.float32) * conv_weight[offset]
        )
    convolved = jax.nn.silu(conv_sum).astype(jnp.bfloat16)
    picks = live_counts[:, None] + jnp.arange(CONV - 1, dtype=jnp.int32)[None, :]
    new_conv = jnp.take_along_axis(padded, picks[:, :, None], axis=1)
    conv_heads = convolved.reshape(local_batch, steps, local_heads, HEAD_DIM)
    branch_heads = branch.reshape(local_batch, steps, local_heads, HEAD_DIM)
    queries = jnp.einsum(
        "blhd,hde->blhe", conv_heads, w_query, preferred_element_type=jnp.float32
    ).astype(jnp.bfloat16)
    key_rows = jnp.einsum(
        "blhd,hde->blhe", conv_heads, w_key, preferred_element_type=jnp.float32
    ).astype(jnp.bfloat16)
    value_rows = jnp.einsum(
        "blhd,hde->blhe", branch_heads, w_value, preferred_element_type=jnp.float32
    ).astype(jnp.bfloat16)
    joined = jnp.concatenate([queries, key_rows, value_rows], axis=-1)
    input_log = (
        jnp.einsum("blhc,hc->blh", joined, w_input_gate, preferred_element_type=jnp.float32)
        + bias_input
    )
    forget_pre = (
        jnp.einsum("blhc,hc->blh", joined, w_forget_gate, preferred_element_type=jnp.float32)
        + bias_forget
    )
    forget_log = jax.nn.log_sigmoid(forget_pre)
    positions = jnp.arange(steps, dtype=jnp.int32)
    live = positions[None, :] < live_counts[:, None]
    input_log = jnp.transpose(jnp.where(live[:, :, None], input_log, very_negative), (0, 2, 1))
    forget_log = jnp.transpose(jnp.where(live[:, :, None], forget_log, 0.0), (0, 2, 1))
    query_heads = jnp.transpose(queries.astype(jnp.float32), (0, 2, 1, 3))
    key_heads = jnp.transpose(key_rows.astype(jnp.float32), (0, 2, 1, 3)) * HEAD_DIM ** (-0.5)
    value_heads = jnp.transpose(value_rows.astype(jnp.float32), (0, 2, 1, 3))
    cumulative = jnp.cumsum(forget_log, axis=-1)
    log_weights = cumulative[..., :, None] - cumulative[..., None, :] + input_log[..., None, :]
    causal = positions[:, None] >= positions[None, :]
    log_weights = jnp.where(causal, log_weights, very_negative)
    carried = cumulative + max_state[..., None]
    stabilizer = jnp.maximum(jnp.max(log_weights, axis=-1), carried)
    weights = jnp.exp(log_weights - stabilizer[..., None])
    carried_scale = jnp.exp(carried - stabilizer)
    scores = jnp.einsum("bhtd,bhsd->bhts", query_heads, key_heads) * weights
    numerator = jnp.einsum("bhts,bhse->bhte", scores, value_heads)
    numerator = numerator + carried_scale[..., None] * jnp.einsum(
        "bhtd,bhde->bhte", query_heads, memory
    )
    centered = numerator - jnp.mean(numerator, axis=-1, keepdims=True)
    normalized = centered * lax.rsqrt(
        jnp.mean(centered * centered, axis=-1, keepdims=True) + epsilon
    )
    normalized = normalized * out_gain[None, :, None, :]
    readout = jnp.transpose(normalized, (0, 2, 1, 3)).reshape(local_batch, steps, local_width)
    new_max = stabilizer[..., -1]
    decay = jnp.exp(cumulative[..., -1] + max_state - new_max)
    update_weight = jnp.exp(cumulative[..., -1:] - cumulative + input_log - new_max[..., None])
    new_memory = decay[..., None, None] * memory + jnp.einsum(
        "bhs,bhsd,bhse->bhde", update_weight, key_heads, value_heads
    )
    mixed = (readout + skip_gain * convolved.astype(jnp.float32)) * jax.nn.silu(
        silu_gate.astype(jnp.float32)
    )
    mixed = jnp.where(live[:, :, None], mixed, 0.0).astype(jnp.bfloat16)
    return (mixed, new_conv, new_memory, new_max)


def layer_step(
    tokens,
    live_counts,
    gain,
    w_branch,
    w_silu_gate,
    conv_weight,
    w_query,
    w_key,
    w_value,
    w_input_gate,
    w_forget_gate,
    bias_input,
    bias_forget,
    out_gain,
    skip_gain,
    w_out,
    conv_state,
    memory,
    max_state,
):
    all_batch = tokens.shape[0]
    steps = tokens.shape[1]
    local_features = tokens.shape[2]
    local_width = w_branch.shape[1]
    local_batch = live_counts.shape[0]
    floats = tokens.astype(jnp.float32)
    partial_squares = jnp.sum(floats * floats, axis=-1)
    total_squares = lax.psum(partial_squares, "dp")
    normed = (floats * lax.rsqrt(total_squares / D + epsilon)[..., None] * gain).astype(
        jnp.bfloat16
    )
    rows = normed.reshape(local_batch * lax.axis_size("dp") * steps, local_features)
    first = jnp.dot(rows, w_branch, preferred_element_type=jnp.float32)
    second = jnp.dot(rows, w_silu_gate, preferred_element_type=jnp.float32)
    summed = lax.psum_scatter(
        jnp.stack([first, second], axis=1)
        .reshape(local_batch * lax.axis_size("dp"), steps, 2, local_width)
        .astype(jnp.bfloat16),
        "dp",
        scatter_dimension=0,
        tiled=True,
    ).astype(jnp.float32)
    branch = summed[:, :, 0].astype(jnp.bfloat16)
    silu_gate = summed[:, :, 1].astype(jnp.bfloat16)
    mixed, new_conv, new_memory, new_max = recurrent_cell(
        branch,
        silu_gate,
        live_counts,
        conv_weight,
        w_query,
        w_key,
        w_value,
        w_input_gate,
        w_forget_gate,
        bias_input,
        bias_forget,
        out_gain,
        skip_gain,
        conv_state,
        memory,
        max_state,
    )
    piece = lax.all_gather(mixed, "dp", axis=0, tiled=True)
    flat = piece.reshape(piece.shape[0] * steps, local_width)
    product = jnp.dot(flat, w_out, preferred_element_type=jnp.float32)
    terms = product.reshape(piece.shape[0], steps, local_features)
    flat_terms = terms.reshape(all_batch * steps, local_features)
    share = lax.psum_scatter(
        flat_terms.astype(jnp.bfloat16), "tp", scatter_dimension=0, tiled=True
    ).astype(jnp.float32)
    share_rows = share.shape[0]
    residual_rows = lax.dynamic_slice_in_dim(
        floats.reshape(all_batch * steps, local_features),
        lax.axis_index("tp") * share_rows,
        share_rows,
        0,
    )
    new_share = (residual_rows + share.astype(jnp.bfloat16).astype(jnp.float32)).astype(
        jnp.bfloat16
    )
    result = lax.all_gather(new_share, "tp", axis=0, tiled=True).reshape(
        all_batch, steps, local_features
    )
    return (result, new_conv, new_memory, new_max)


def per_device(
    tokens,
    live_counts,
    norm_gain,
    w_branch,
    w_silu_gate,
    conv_weight,
    w_query,
    w_key,
    w_value,
    w_input_gate,
    w_forget_gate,
    bias_input,
    bias_forget,
    out_gain,
    skip_gain,
    w_out,
    conv_state,
    memory,
    max_state,
):
    stream = tokens
    conv_list = []
    memory_list = []
    max_list = []
    for which_layer in range(LAYERS):
        stream, new_conv, new_memory, new_max = layer_step(
            stream,
            live_counts,
            norm_gain[which_layer],
            w_branch[which_layer],
            w_silu_gate[which_layer],
            conv_weight[which_layer],
            w_query[which_layer],
            w_key[which_layer],
            w_value[which_layer],
            w_input_gate[which_layer],
            w_forget_gate[which_layer],
            bias_input[which_layer],
            bias_forget[which_layer],
            out_gain[which_layer],
            skip_gain[which_layer],
            w_out[which_layer],
            conv_state[which_layer],
            memory[which_layer],
            max_state[which_layer],
        )
        conv_list.append(new_conv)
        memory_list.append(new_memory)
        max_list.append(new_max)
    return (stream, jnp.stack(conv_list), jnp.stack(memory_list), jnp.stack(max_list))


def solution(mesh):
    in_specs = (
        P("grp", None, "dp"),
        P(("grp", "dp")),
        P(None, "dp"),
        P(None, "dp", "tp"),
        P(None, "dp", "tp"),
        P(None, None, "tp"),
        P(None, "tp", None, None),
        P(None, "tp", None, None),
        P(None, "tp", None, None),
        P(None, "tp", None),
        P(None, "tp", None),
        P(None, "tp"),
        P(None, "tp"),
        P(None, "tp", None),
        P(None, "tp"),
        P(None, "tp", "dp"),
        P(None, ("grp", "dp"), None, "tp"),
        P(None, ("grp", "dp"), "tp", None, None),
        P(None, ("grp", "dp"), "tp"),
    )
    out_specs = (
        P("grp", None, "dp"),
        P(None, ("grp", "dp"), None, "tp"),
        P(None, ("grp", "dp"), "tp", None, None),
        P(None, ("grp", "dp"), "tp"),
    )
    return jax.shard_map(
        per_device, mesh=mesh, in_specs=in_specs, out_specs=out_specs, check_vma=False
    )
```

profile of v0, /device:TPU:0, one launch (start us, length us, event | category | flops | bytes accessed | tf_op | source)
XLA Modules:
  0.0 297.1 jit_solution(8914190688373300822)
XLA Ops:
  7.2 1.4 fusion.162
  9.9 12.9 %psum.14 = f32[64,8]{1,0:T(8,128)S(1)} all-reduce(f32[64,8]{1,0:T(8,128)S(1)} %fusion.16), channel_id=1, replica_groups=mesh['grp'=2,'tp'=4,'dp'=4] {'dp'}, use_global_device_ids=true, to_apply=%region_1.0 | all-reduce | flops 512 | bytes 4096 | tf_op jit(solution)/shard_map/psum | solution.py:133
  22.8 2.1 fusion.11
  26.2 2.5 copy.279
  34.3 26.1 %reduce-scatter.15.cloned.1.call-done = bf16[16,16384]{1,0:T(8,128)(2,1)} async-done(((bf16[64,16384]{1,0:T(8,128)(2,1)}), bf16[16,16384]{1,0:T(8,128)(2,1)}) %reduce-scatter.15.cloned.1.call-update) | async-done | bytes 524304
  60.5 1.4 copy.280
  65.6 1.8 fusion.76
  67.4 1.8 fusion.77
  69.4 2.8 reduce_window_sum.17
  75.2 7.0 %fusion.4 = f32[16,4,8,256]{3,2,1,0:T(8,128)S(1)} fusion(f32[2,16,4,256,256]{4,3,2,1,0:T(8,128)} %param.38, bf16[4,16,8,256]{3,2,1,0:T(8,128)(2,1)S(1)} %convolution_convert_fusion.11), kind=kOutput, calls=%fused_computation.9 | convolution fusion | flops 67108864 | bytes 9175040 | tf_op jit(solution)/shard_map/bhtd,bhde->bhte/dot_general | solution.py:83
  85.8 16.8 %all-gather.3.cloned.1.call-done = bf16[64,8,1024]{2,1,0:T(8,128)(2,1)} async-done(((bf16[16,8,1024]{2,1,0:T(8,128)(2,1)}), bf16[64,8,1024]{2,1,0:T(8,128)(2,1)}) %all-gather.3.cloned.1.call-update) | async-done | bytes 1048592 | tf_op jit(solution)/shard_map/all_gather | solution.py:168
  102.6 3.0 %convolution_convert_fusion.5 = bf16[512,512]{1,0:T(8,128)(2,1)} fusion(bf16[64,8,1024]{2,1,0:T(8,128)(2,1)} %all-gather.3.cloned.1.call-done, bf16[2,1024,512]{2,1,0:T(8,128)(2,1)} %param.36), kind=kOutput, calls=%fused_computation.29 | convolution fusion | flops 537133056 | bytes 2621440 | tf_op jit(solution)/shard_map/dot_general | solution.py:170
  105.8 21.8 %reduce-scatter.11.cloned.1.call-done = bf16[128,512]{1,0:T(8,128)(2,1)} async-done(((bf16[512,512]{1,0:T(8,128)(2,1)}), bf16[128,512]{1,0:T(8,128)(2,1)}) %reduce-scatter.11.cloned.1.call-update) | async-done | bytes 131088 | tf_op jit(solution)/shard_map/reduce_scatter | solution.py:173
  128.6 15.6 %all_gather.13 = bf16[512,512]{1,0:T(8,128)(2,1)S(1)} all-gather(bf16[128,512]{1,0:T(8,128)(2,1)S(1)} %add_convert_fusion.1), channel_id=1, replica_groups=mesh['grp'=2,'tp'=4,'dp'=4] {'tp'}, dimensions={0}, use_global_device_ids=true | all-gather | bytes 655360 | tf_op jit(solution)/shard_map/all_gather | solution.py:186
  144.4 10.3 %psum.15 = f32[64,8]{1,0:T(8,128)S(1)} all-reduce(f32[64,8]{1,0:T(8,128)S(1)} %reduce_sum.60), channel_id=1, replica_groups=mesh['grp'=2,'tp'=4,'dp'=4] {'dp'}, use_global_device_ids=true, to_apply=%region_9.10 | all-reduce | flops 512 | bytes 4096 | tf_op jit(solution)/shard_map/psum | solution.py:133
  154.8 2.0 fusion.13
  156.8 2.0 fusion.12
  159.2 2.5 copy.281
  163.5 28.2 %reduce-scatter.17.cloned.1.call-done = bf16[16,16384]{1,0:T(8,128)(2,1)} async-done(((bf16[64,16384]{1,0:T(8,128)(2,1)}), bf16[16,16384]{1,0:T(8,128)(2,1)}) %reduce-scatter.17.cloned.1.call-update) | async-done | bytes 524304
  196.8 1.4 convolution_convert_fusion.7
  198.2 1.5 convolution_convert_fusion.6
  199.8 1.8 fusion.74
  201.6 1.8 fusion.75
  203.6 2.8 reduce_window_sum.18
  207.1 7.1 %fusion = f32[16,4,8,256]{3,2,1,0:T(8,128)S(1)} fusion(f32[2,16,4,256,256]{4,3,2,1,0:T(8,128)} %param.38, bf16[4,16,8,256]{3,2,1,0:T(8,128)(2,1)} %copy-done.1), kind=kOutput, calls=%fused_computation.4 | convolution fusion | flops 67108864 | bytes 9175040 | tf_op jit(solution)/shard_map/bhtd,bhde->bhte/dot_general | solution.py:83
  218.7 1.7 bitcast_multiply_fusion.3
  220.4 1.5 fusion.109
  225.1 10.8 %fusion.3 = f32[1,16,4,256,256]{4,3,2,1,0:T(8,128)} fusion(f32[2,16,4,256,256]{4,3,2,1,0:T(8,128)} %param.38, f32[16,4]{1,0:T(8,128)S(1)} %copy.242, bf16[16,4,8,256]{3,2,0,1:T(8,128)(2,1)S(1)} %get-tuple-element.27, bf16[4,16,8,256]{3,2,1,0:T(8,128)(2,1)S(1)} %copy-done.9), kind=kOutput, calls=%fused_computation.7 | convolution fusion | flops 75497472 | bytes 34078976 | tf_op jit(solution)/shard_map/bhs,bhsd,bhse->bhde/dot_general | solution.py:95
  236.0 10.8 %fusion.7 = f32[1,16,4,256,256]{4,3,2,1,0:T(8,128)} fusion(f32[2,16,4,256,256]{4,3,2,1,0:T(8,128)} %param.38, f32[16,4]{1,0:T(8,128)S(1)} %copy.234, bf16[16,4,8,256]{3,2,0,1:T(8,128)(2,1)S(1)} %get-tuple-element.25, bf16[4,16,8,256]{3,2,1,0:T(8,128)(2,1)S(1)} %copy-done.7), kind=kOutput, calls=%fused_computation.12 | convolution fusion | flops 75497472 | bytes 34078976 | tf_op jit(solution)/shard_map/bhs,bhsd,bhse->bhde/dot_general | solution.py:95
  246.8 3.0 %convolution_convert_fusion.4 = bf16[512,512]{1,0:T(8,128)(2,1)} fusion(bf16[64,8,1024]{2,1,0:T(8,128)(2,1)} %all-gather.5.cloned.1.call-done, bf16[2,1024,512]{2,1,0:T(8,128)(2,1)} %param.36), kind=kOutput, calls=%fused_computation.28 | convolution fusion | flops 537133056 | bytes 2621440 | tf_op jit(solution)/shard_map/dot_general | solution.py:170
  249.9 23.1 %pad_maximum_fusion = f32[2,16,4,256,256]{4,3,2,1,0:T(8,128)} fusion(f32[1,16,4,256,256]{4,3,2,1,0:T(8,128)} %fusion.3, f32[1,16,4,256,256]{4,3,2,1,0:T(8,128)} %fusion.7), kind=kLoop, calls=%fused_computation.2 | loop fusion | flops 8388608 | bytes 67108864 | tf_op jit(solution)/shard_map/stack | solution.py:242
  273.9 15.6 %all_gather.15 = bf16[512,512]{1,0:T(8,128)(2,1)S(1)} all-gather(bf16[128,512]{1,0:T(8,128)(2,1)S(1)} %add_convert_fusion), channel_id=1, replica_groups=mesh['grp'=2,'tp'=4,'dp'=4] {'tp'}, dimensions={0}, use_global_device_ids=true | all-gather | bytes 655360 | tf_op jit(solution)/shard_map/all_gather | solution.py:186
  (216 shorter events, 37.0 us)
Async XLA Ops:
  7.2 17.8 %copy-start = (bf16[64,8,512]{2,1,0:T(8,128)(2,1)S(1)}, bf16[64,8,512]{2,1,0:T(8,128)(2,1)}, u32[]{:S(2)}) copy-start(bf16[64,8,512]{2,1,0:T(8,128)(2,1)} %param.21) | copy-start | bytes 1572868
  7.2 17.8 %copy-start.47 = (bf16[2,512,1024]{2,1,0:T(8,128)(2,1)S(1)}, bf16[2,512,1024]{2,1,0:T(8,128)(2,1)}, u32[]{:S(2)}) copy-start(bf16[2,512,1024]{2,1,0:T(8,128)(2,1)} %param.24) | copy-start | bytes 6291460
  7.2 53.3 %reduce-scatter.15.cloned.1.call-start = ((), (), s32[]{:S(2)}) async-start(), calls=%async_computation.8 | async-start | bytes 2621440
  28.7 3.7 %copy-start.26 = (bf16[2,4,768]{2,1,0:T(4,128)(2,1)S(1)}, bf16[2,4,768]{2,1,0:T(4,128)(2,1)}, u32[]{:S(2)}) copy-start(bf16[2,4,768]{2,1,0:T(4,128)(2,1)} %param.30) | copy-start | bytes 36868
  28.7 4.3 %copy-start.27 = (bf16[2,4,768]{2,1,0:T(4,128)(2,1)S(1)}, bf16[2,4,768]{2,1,0:T(4,128)(2,1)}, u32[]{:S(2)}) copy-start(bf16[2,4,768]{2,1,0:T(4,128)(2,1)} %param.31) | copy-start | bytes 36868
  28.8 4.9 %copy-start.14 = (f32[2,4,1024]{2,1,0:T(4,128)S(1)}, f32[2,4,1024]{2,1,0:T(4,128)}, u32[]{:S(2)}) copy-start(f32[2,4,1024]{2,1,0:T(4,128)} %param.26) | copy-start | bytes 98308
  28.8 5.5 %copy-start.11 = (bf16[2,16,3,1024]{3,1,2,0:T(8,128)(2,1)S(1)}, bf16[2,16,3,1024]{3,1,2,0:T(8,128)(2,1)}, u32[]{:S(2)}) copy-start(bf16[2,16,3,1024]{3,1,2,0:T(8,128)(2,1)} %param.37) | copy-start | bytes 589828
  28.8 73.8 %all-gather.3.cloned.1.call-start = ((), (), s32[]{:S(2)}) async-start(), calls=%async_computation.4 | async-start | bytes 1310720 | tf_op jit(solution)/shard_map/all_gather | solution.py:168
  29.4 32.5 %copy-start.28 = (pred[16,8]{0,1:T(8,128)(4,1)}, pred[16,8]{0,1:T(8,128)(4,1)S(1)}, u32[]{:S(2)}) copy-start(pred[16,8]{0,1:T(8,128)(4,1)S(1)} %iota_compare_fusion.1) | copy-start | bytes 388
  30.1 42.2 %copy-start.39 = (pred[8,8]{1,0:T(8,128)(4,1)}, pred[8,8]{1,0:T(8,128)(4,1)S(1)}, u32[]{:S(2)}) copy-start(pred[8,8]{1,0:T(8,128)(4,1)S(1)} %iota_compare_fusion) | copy-start | bytes 196
  30.7 41.6 %copy-start.38 = (f32[4]{0:T(128)}, f32[4]{0:T(128)S(1)}, u32[]{:S(2)}) copy-start(f32[4]{0:T(128)S(1)} %get-tuple-element.66) | copy-start | bytes 52
  65.6 16.6 %copy-start.6 = (bf16[4,16,8,256]{3,2,1,0:T(8,128)(2,1)}, bf16[4,16,8,256]{3,2,1,0:T(8,128)(2,1)S(1)}, u32[]{:S(2)}) copy-start(bf16[4,16,8,256]{3,2,1,0:T(8,128)(2,1)S(1)} %convolution_convert_fusion.9) | copy-start | bytes 786436
  73.5 8.7 %copy-start.15 = (f32[16,4,1]{0,1,2:T(4,128)}, f32[16,4,1]{0,1,2:T(4,128)S(1)}, u32[]{:S(2)}) copy-start(f32[16,4,1]{0,1,2:T(4,128)S(1)} %copy.232) | copy-start | bytes 772
  75.2 7.0 %copy-start.13 = (f32[16,4,8]{2,1,0:T(4,128)S(1)}, f32[16,4,8]{2,1,0:T(4,128)}, u32[]{:S(2)}) copy-start(f32[16,4,8]{2,1,0:T(4,128)} %copy-done.12) | copy-start | bytes 6148
  85.7 41.9 %reduce-scatter.11.cloned.1.call-start = ((), (), s32[]{:S(2)}) async-start(), calls=%async_computation.5 | async-start | bytes 655360 | tf_op jit(solution)/shard_map/reduce_scatter | solution.py:173
  105.6 49.1 %copy-start.42 = (f32[1,512]{1,0:T(1,128)S(1)}, f32[1,512]{1,0:T(1,128)}, u32[]{:S(2)}) copy-start(f32[1,512]{1,0:T(1,128)} %get-tuple-element.60) | copy-start | bytes 6148
  105.6 86.0 %reduce-scatter.17.cloned.1.call-start = ((), (), s32[]{:S(2)}) async-start(), calls=%async_computation.9 | async-start | bytes 2621440
  161.7 85.1 %all-gather.5.cloned.1.call-start = ((), (), s32[]{:S(2)}) async-start(), calls=%async_computation.6 | async-start | bytes 1310720 | tf_op jit(solution)/shard_map/all_gather | solution.py:168
  191.6 3.2 %copy-start.20 = (f32[1,1,1024]{2,1,0:T(1,128)S(1)}, f32[1,1,1024]{2,1,0:T(1,128)}, u32[]{:S(2)}) copy-start(f32[1,1,1024]{2,1,0:T(1,128)} %get-tuple-element.44) | copy-start | bytes 12292
  195.1 4.6 %copy-start.35 = (bf16[4,768,1,1]{1,0,2,3:T(4,128)(2,1)S(1)}, bf16[4,768,1,1]{1,0,2,3:T(4,128)(2,1)}, u32[]{:S(2)}) copy-start(bf16[4,768,1,1]{1,0,2,3:T(4,128)(2,1)} %get-tuple-element.49) | copy-start | bytes 18436
  196.7 4.8 %copy-start.1 = (bf16[4,16,8,256]{3,2,1,0:T(8,128)(2,1)}, bf16[4,16,8,256]{3,2,1,0:T(8,128)(2,1)S(1)}, u32[]{:S(2)}) copy-start(bf16[4,16,8,256]{3,2,1,0:T(8,128)(2,1)S(1)} %convolution_convert_fusion.8) | copy-start | bytes 786436
  198.2 5.2 %copy-start.4 = (bf16[4,16,8,256]{3,2,1,0:T(8,128)(2,1)}, bf16[4,16,8,256]{3,2,1,0:T(8,128)(2,1)S(1)}, u32[]{:S(2)}) copy-start(bf16[4,16,8,256]{3,2,1,0:T(8,128)(2,1)S(1)} %convolution_convert_fusion.7) | copy-start | bytes 786436
  198.2 3.4 %copy-start.36 = (bf16[4,768,1,1]{1,0,2,3:T(4,128)(2,1)S(1)}, bf16[4,768,1,1]{1,0,2,3:T(4,128)(2,1)}, u32[]{:S(2)}) copy-start(bf16[4,768,1,1]{1,0,2,3:T(4,128)(2,1)} %get-tuple-element.47) | copy-start | bytes 18436
  199.7 3.7 %copy-start.8 = (bf16[4,16,8,256]{3,2,1,0:T(8,128)(2,1)}, bf16[4,16,8,256]{3,2,1,0:T(8,128)(2,1)S(1)}, u32[]{:S(2)}) copy-start(bf16[4,16,8,256]{3,2,1,0:T(8,128)(2,1)S(1)} %convolution_convert_fusion.6) | copy-start | bytes 786436
  199.7 3.7 %copy-start.41 = (f32[4]{0:T(128)S(1)}, f32[4]{0:T(128)}, u32[]{:S(2)}) copy-start(f32[4]{0:T(128)} %get-tuple-element.63) | copy-start | bytes 52
  199.7 6.7 %copy-start.37 = (f32[4]{0:T(128)S(1)}, f32[4]{0:T(128)}, u32[]{:S(2)}) copy-start(f32[4]{0:T(128)} %get-tuple-element.65) | copy-start | bytes 52
  199.8 6.7 %copy-start.40 = (pred[8,8]{1,0:T(8,128)(4,1)S(1)}, pred[8,8]{1,0:T(8,128)(4,1)}, u32[]{:S(2)}) copy-start(pred[8,8]{1,0:T(8,128)(4,1)} %copy-done.39) | copy-start | bytes 196
  214.1 4.1 %copy-start.16 = (f32[16,4,1]{0,1,2:T(4,128)S(1)}, f32[16,4,1]{0,1,2:T(4,128)}, u32[]{:S(2)}) copy-start(f32[16,4,1]{0,1,2:T(4,128)} %copy-done.15) | copy-start | bytes 772
  214.2 4.1 %copy-start.25 = (f32[2,16,4]{1,2,0:T(4,128)S(1)}, f32[2,16,4]{1,2,0:T(4,128)}, u32[]{:S(2)}) copy-start(f32[2,16,4]{1,2,0:T(4,128)} %param.39) | copy-start | bytes 1540
  215.4 5.0 %copy-start.2 = (bf16[4,16,8,256]{3,2,1,0:T(8,128)(2,1)S(1)}, bf16[4,16,8,256]{3,2,1,0:T(8,128)(2,1)}, u32[]{:S(2)}) copy-start(bf16[4,16,8,256]{3,2,1,0:T(8,128)(2,1)} %copy-done.1) | copy-start | bytes 786436
  224.3 48.7 %reduce-scatter.13.cloned.1.call-start = ((), (), s32[]{:S(2)}) async-start(), calls=%async_computation.7 | async-start | bytes 655360 | tf_op jit(solution)/shard_map/reduce_scatter | solution.py:173
  225.1 10.9 %copy-start.7 = (bf16[4,16,8,256]{3,2,1,0:T(8,128)(2,1)S(1)}, bf16[4,16,8,256]{3,2,1,0:T(8,128)(2,1)}, u32[]{:S(2)}) copy-start(bf16[4,16,8,256]{3,2,1,0:T(8,128)(2,1)} %copy-done.6) | copy-start | bytes 786436
  (24 other events, 44.8 us)
Sparse Core Ops, SparseCore 0:
  28.9 31.4 reduce-scatter.14
  85.8 16.6 all-gather.2
  105.8 21.8 reduce-scatter.10
  161.9 29.7 reduce-scatter.16
  224.4 16.7 all-gather.4
  250.0 21.9 reduce-scatter.12
where the time goes:
time: 298 us; the launch traced here: 297 us
  waiting for transfers between devices  93 us (31%)
  matrix products  65.3 us (22%)
  blocking collectives  54.3 us (18%)
  other arithmetic  41.4 us (14%)
  local copies, waits for them, and re-layouts  27.7 us (9%)
  between operations  15 us (5%)
    unnamed x8, waiting for transfers between devices  54.4 us
    all_gather x2, blocking collectives, layer_step(): lax.all_gather(new_share, 'tp', axis=0, tiled=True)  31.1 us
    psum x2, blocking collectives, layer_step(): total_squares = lax.psum(partial_squares, 'dp')  23.2 us
    another operation x1, other arithmetic, per_device(): jnp.stack(memory_list)  23.1 us
    reduce_scatter x2, waiting for transfers between devices, layer_step(): lax.psum_scatter(flat_terms.astype(jnp.bfloat16), 'tp', scatter_dimension...  21.8 us
    dot_general x2, matrix products, recurrent_cell(): jnp.einsum('bhs,bhsd,bhse->bhde', update_weight, key_heads, value_heads)  21.7 us
    all_gather x2, waiting for transfers between devices, layer_step(): piece = lax.all_gather(mixed, 'dp', axis=0, tiled=True)  16.8 us
    dot_general x2, matrix products, recurrent_cell(): jnp.einsum('bhtd,bhde->bhte', query_heads, memory)  14 us
  transfers between devices with their start and end apart: 6, of which 4 were waited for; matrix products, arithmetic and copies ran while one was open for 17% of the time, Pallas kernels for 0%

commit v1 on v0

--- a/solution.py
+++ b/solution.py
@@ -130,7 +130,7 @@
     local_batch = live_counts.shape[0]
     floats = tokens.astype(jnp.float32)
     partial_squares = jnp.sum(floats * floats, axis=-1)
-    total_squares = lax.psum(partial_squares, "dp")
+    total_squares = jnp.sum(lax.all_gather(partial_squares, "dp"), axis=0)
     normed = (floats * lax.rsqrt(total_squares / D + epsilon)[..., None] * gain).astype(
         jnp.bfloat16
     )

time: 298 us -> 289 us (0.970)
  blocking collectives: 54.3 us -> 42.6 us
    psum x2 -> x0, blocking collectives: 23.2 us -> none  [layer_step(): total_squares = lax.psum(partial_squares, 'dp')]
    all_gather x0 -> x2, blocking collectives: none -> 11.4 us  [layer_step(): total_squares = jnp.sum(lax.all_gather(partial_squares, 'dp'), axis=0)]
    unnamed x110 -> x107, local copies, waits for them, and re-layouts: 11.9 us -> 11.9 us
  transfers between devices with their start and end apart: 6 -> 6, of which waited for: 4 -> 4; matrix products, arithmetic and copies ran while one was open for 17% -> 18% of each run, Pallas kernels for 0% -> 0%
where the time goes in v1:
time: 289 us; the launch traced here: 288 us
  waiting for transfers between devices  94.2 us (33%)
  matrix products  66.4 us (23%)
  blocking collectives  42.6 us (15%)
  other arithmetic  41.3 us (14%)
  local copies, waits for them, and re-layouts  28 us (10%)
  between operations  14.9 us (5%)
    unnamed x8, waiting for transfers between devices  55.6 us
    all_gather x2, blocking collectives, layer_step(): lax.all_gather(new_share, 'tp', axis=0, tiled=True)  31.2 us
    another operation x1, other arithmetic, per_device(): jnp.stack(memory_list)  23.1 us
    reduce_scatter x2, waiting for transfers between devices, layer_step(): lax.psum_scatter(flat_terms.astype(jnp.bfloat16), 'tp', scatter_dimension...  21.8 us
    dot_general x2, matrix products, recurrent_cell(): jnp.einsum('bhs,bhsd,bhse->bhde', update_weight, key_heads, value_heads)  21.7 us
    all_gather x2, waiting for transfers between devices, layer_step(): piece = lax.all_gather(mixed, 'dp', axis=0, tiled=True)  16.8 us
    dot_general x2, matrix products, recurrent_cell(): jnp.einsum('bhtd,bhde->bhte', query_heads, memory)  14 us
    unnamed x107, local copies, waits for them, and re-layouts  11.9 us
  transfers between devices with their start and end apart: 6, of which 4 were waited for; matrix products, arithmetic and copies ran while one was open for 18% of the time, Pallas kernels for 0%

profile of v1, /device:TPU:0, one launch (start us, length us, event | category | flops | bytes accessed | tf_op | source)
XLA Modules:
  0.0 287.9 jit_solution(6003115910297184096)
XLA Ops:
  7.2 1.4 fusion.162
  10.0 6.2 %all-gather.1 = f32[4,64,8]{1,2,0:T(8,128)S(1)} all-gather(f32[1,64,8]{1,2,0:T(8,128)S(1)} %copy.257), channel_id=2, replica_groups=mesh['grp'=2,'tp'=4,'dp'=4] {'dp'}, dimensions={0}, use_global_device_ids=true | all-gather | bytes 10240 | tf_op jit(solution)/shard_map/all_gather | solution.py:133
  16.3 2.1 fusion.11
  19.7 2.5 copy.340
  27.8 27.5 %reduce-scatter.15.cloned.1.call-done = bf16[16,16384]{1,0:T(8,128)(2,1)} async-done(((bf16[64,16384]{1,0:T(8,128)(2,1)}), bf16[16,16384]{1,0:T(8,128)(2,1)}) %reduce-scatter.15.cloned.1.call-update) | async-done | bytes 524304
  55.3 1.4 copy.341
  59.9 1.6 convolution_convert_fusion.9
  61.5 1.8 fusion.76
  63.3 1.8 fusion.77
  65.3 2.8 reduce_window_sum.17
  71.0 7.0 %fusion.4 = f32[16,4,8,256]{3,2,1,0:T(8,128)S(1)} fusion(f32[2,16,4,256,256]{4,3,2,1,0:T(8,128)} %param.38, bf16[4,16,8,256]{3,2,1,0:T(8,128)(2,1)S(1)} %convolution_convert_fusion.11), kind=kOutput, calls=%fused_computation.9 | convolution fusion | flops 67108864 | bytes 9175040 | tf_op jit(solution)/shard_map/bhtd,bhde->bhte/dot_general | solution.py:83
  81.6 16.8 %all-gather.5.cloned.1.call-done = bf16[64,8,1024]{2,1,0:T(8,128)(2,1)} async-done(((bf16[16,8,1024]{2,1,0:T(8,128)(2,1)}), bf16[64,8,1024]{2,1,0:T(8,128)(2,1)}) %all-gather.5.cloned.1.call-update) | async-done | bytes 1048592 | tf_op jit(solution)/shard_map/all_gather | solution.py:168
  98.4 3.0 %convolution_convert_fusion.5 = bf16[512,512]{1,0:T(8,128)(2,1)} fusion(bf16[64,8,1024]{2,1,0:T(8,128)(2,1)} %all-gather.5.cloned.1.call-done, bf16[2,1024,512]{2,1,0:T(8,128)(2,1)} %param.36), kind=kOutput, calls=%fused_computation.29 | convolution fusion | flops 537133056 | bytes 2621440 | tf_op jit(solution)/shard_map/dot_general | solution.py:170
  101.7 21.8 %reduce-scatter.11.cloned.1.call-done = bf16[128,512]{1,0:T(8,128)(2,1)} async-done(((bf16[512,512]{1,0:T(8,128)(2,1)}), bf16[128,512]{1,0:T(8,128)(2,1)}) %reduce-scatter.11.cloned.1.call-update) | async-done | bytes 131088 | tf_op jit(solution)/shard_map/reduce_scatter | solution.py:173
  124.4 15.6 %all_gather.27 = bf16[512,512]{1,0:T(8,128)(2,1)S(1)} all-gather(bf16[128,512]{1,0:T(8,128)(2,1)S(1)} %add_convert_fusion.1), channel_id=1, replica_groups=mesh['grp'=2,'tp'=4,'dp'=4] {'tp'}, dimensions={0}, use_global_device_ids=true | all-gather | bytes 655360 | tf_op jit(solution)/shard_map/all_gather | solution.py:186
  140.4 5.2 %all_gather.29 = f32[4,64,8]{1,2,0:T(8,128)S(1)} all-gather(f32[1,64,8]{1,2,0:T(8,128)S(1)} %copy.274), channel_id=1, replica_groups=mesh['grp'=2,'tp'=4,'dp'=4] {'dp'}, dimensions={0}, use_global_device_ids=true | all-gather | bytes 10240 | tf_op jit(solution)/shard_map/all_gather | solution.py:133
  145.8 2.0 fusion.13
  147.8 2.0 fusion.12
  150.2 2.5 copy.342
  154.5 27.9 %reduce-scatter.17.cloned.1.call-done = bf16[16,16384]{1,0:T(8,128)(2,1)} async-done(((bf16[64,16384]{1,0:T(8,128)(2,1)}), bf16[16,16384]{1,0:T(8,128)(2,1)}) %reduce-scatter.17.cloned.1.call-update) | async-done | bytes 524304
  189.0 1.5 convolution_convert_fusion.6
  190.5 1.8 fusion.74
  192.3 1.8 fusion.75
  194.4 2.8 reduce_window_sum.18
  197.8 7.1 %fusion = f32[16,4,8,256]{3,2,1,0:T(8,128)S(1)} fusion(f32[2,16,4,256,256]{4,3,2,1,0:T(8,128)} %param.38, bf16[4,16,8,256]{3,2,1,0:T(8,128)(2,1)} %copy-done.1), kind=kOutput, calls=%fused_computation.4 | convolution fusion | flops 67108864 | bytes 9175040 | tf_op jit(solution)/shard_map/bhtd,bhde->bhte/dot_general | solution.py:83
  209.4 1.7 bitcast_multiply_fusion.3
  211.2 1.5 fusion.109
  215.9 10.9 %fusion.3 = f32[1,16,4,256,256]{4,3,2,1,0:T(8,128)} fusion(f32[2,16,4,256,256]{4,3,2,1,0:T(8,128)} %param.38, f32[16,4]{1,0:T(8,128)S(1)} %copy.303, bf16[16,4,8,256]{3,2,0,1:T(8,128)(2,1)S(1)} %get-tuple-element.31, bf16[4,16,8,256]{3,2,1,0:T(8,128)(2,1)S(1)} %copy-done.9), kind=kOutput, calls=%fused_computation.7 | convolution fusion | flops 75497472 | bytes 34078976 | tf_op jit(solution)/shard_map/bhs,bhsd,bhse->bhde/dot_general | solution.py:95
  226.8 10.8 %fusion.7 = f32[1,16,4,256,256]{4,3,2,1,0:T(8,128)} fusion(f32[2,16,4,256,256]{4,3,2,1,0:T(8,128)} %param.38, f32[16,4]{1,0:T(8,128)S(1)} %copy.295, bf16[16,4,8,256]{3,2,0,1:T(8,128)(2,1)S(1)} %get-tuple-element.29, bf16[4,16,8,256]{3,2,1,0:T(8,128)(2,1)S(1)} %copy-done.7), kind=kOutput, calls=%fused_computation.12 | convolution fusion | flops 75497472 | bytes 34078976 | tf_op jit(solution)/shard_map/bhs,bhsd,bhse->bhde/dot_general | solution.py:95
  237.6 3.0 %convolution_convert_fusion.4 = bf16[512,512]{1,0:T(8,128)(2,1)} fusion(bf16[64,8,1024]{2,1,0:T(8,128)(2,1)} %all-gather.7.cloned.1.call-done, bf16[2,1024,512]{2,1,0:T(8,128)(2,1)} %param.36), kind=kOutput, calls=%fused_computation.28 | convolution fusion | flops 537133056 | bytes 2621440 | tf_op jit(solution)/shard_map/dot_general | solution.py:170
  240.7 23.1 %pad_maximum_fusion = f32[2,16,4,256,256]{4,3,2,1,0:T(8,128)} fusion(f32[1,16,4,256,256]{4,3,2,1,0:T(8,128)} %fusion.3, f32[1,16,4,256,256]{4,3,2,1,0:T(8,128)} %fusion.7), kind=kLoop, calls=%fused_computation.2 | loop fusion | flops 8388608 | bytes 67108864 | tf_op jit(solution)/shard_map/stack | solution.py:242
  264.7 15.6 %all_gather.31 = bf16[512,512]{1,0:T(8,128)(2,1)S(1)} all-gather(bf16[128,512]{1,0:T(8,128)(2,1)S(1)} %add_convert_fusion), channel_id=1, replica_groups=mesh['grp'=2,'tp'=4,'dp'=4] {'tp'}, dimensions={0}, use_global_device_ids=true | all-gather | bytes 655360 | tf_op jit(solution)/shard_map/all_gather | solution.py:186
  (218 shorter events, 38.1 us)
Async XLA Ops:
  7.2 11.3 %copy-start = (bf16[64,8,512]{2,1,0:T(8,128)(2,1)S(1)}, bf16[64,8,512]{2,1,0:T(8,128)(2,1)}, u32[]{:S(2)}) copy-start(bf16[64,8,512]{2,1,0:T(8,128)(2,1)} %param.21) | copy-start | bytes 1572868
  7.2 11.3 %copy-start.46 = (bf16[2,512,1024]{2,1,0:T(8,128)(2,1)S(1)}, bf16[2,512,1024]{2,1,0:T(8,128)(2,1)}, u32[]{:S(2)}) copy-start(bf16[2,512,1024]{2,1,0:T(8,128)(2,1)} %param.24) | copy-start | bytes 6291460
  7.2 48.1 %reduce-scatter.15.cloned.1.call-start = ((), (), s32[]{:S(2)}) async-start(), calls=%async_computation.8 | async-start | bytes 2621440
  22.2 3.7 %copy-start.25 = (bf16[2,4,768]{2,1,0:T(4,128)(2,1)S(1)}, bf16[2,4,768]{2,1,0:T(4,128)(2,1)}, u32[]{:S(2)}) copy-start(bf16[2,4,768]{2,1,0:T(4,128)(2,1)} %param.30) | copy-start | bytes 36868
  22.2 4.3 %copy-start.26 = (bf16[2,4,768]{2,1,0:T(4,128)(2,1)S(1)}, bf16[2,4,768]{2,1,0:T(4,128)(2,1)}, u32[]{:S(2)}) copy-start(bf16[2,4,768]{2,1,0:T(4,128)(2,1)} %param.31) | copy-start | bytes 36868
  22.3 4.9 %copy-start.13 = (f32[2,4,1024]{2,1,0:T(4,128)S(1)}, f32[2,4,1024]{2,1,0:T(4,128)}, u32[]{:S(2)}) copy-start(f32[2,4,1024]{2,1,0:T(4,128)} %param.26) | copy-start | bytes 98308
  22.3 5.5 %copy-start.10 = (bf16[2,16,3,1024]{3,1,2,0:T(8,128)(2,1)S(1)}, bf16[2,16,3,1024]{3,1,2,0:T(8,128)(2,1)}, u32[]{:S(2)}) copy-start(bf16[2,16,3,1024]{3,1,2,0:T(8,128)(2,1)} %param.37) | copy-start | bytes 589828
  22.3 76.1 %all-gather.5.cloned.1.call-start = ((), (), s32[]{:S(2)}) async-start(), calls=%async_computation.4 | async-start | bytes 1310720 | tf_op jit(solution)/shard_map/all_gather | solution.py:168
  22.9 33.9 %copy-start.27 = (pred[16,8]{0,1:T(8,128)(4,1)}, pred[16,8]{0,1:T(8,128)(4,1)S(1)}, u32[]{:S(2)}) copy-start(pred[16,8]{0,1:T(8,128)(4,1)S(1)} %iota_compare_fusion.1) | copy-start | bytes 388
  23.6 44.6 %copy-start.38 = (pred[8,8]{1,0:T(8,128)(4,1)}, pred[8,8]{1,0:T(8,128)(4,1)S(1)}, u32[]{:S(2)}) copy-start(pred[8,8]{1,0:T(8,128)(4,1)S(1)} %iota_compare_fusion) | copy-start | bytes 196
  24.2 44.0 %copy-start.37 = (f32[4]{0:T(128)}, f32[4]{0:T(128)S(1)}, u32[]{:S(2)}) copy-start(f32[4]{0:T(128)S(1)} %get-tuple-element.70) | copy-start | bytes 52
  61.5 16.5 %copy-start.6 = (bf16[4,16,8,256]{3,2,1,0:T(8,128)(2,1)}, bf16[4,16,8,256]{3,2,1,0:T(8,128)(2,1)S(1)}, u32[]{:S(2)}) copy-start(bf16[4,16,8,256]{3,2,1,0:T(8,128)(2,1)S(1)} %convolution_convert_fusion.9) | copy-start | bytes 786436
  69.4 8.6 %copy-start.14 = (f32[16,4,1]{0,1,2:T(4,128)}, f32[16,4,1]{0,1,2:T(4,128)S(1)}, u32[]{:S(2)}) copy-start(f32[16,4,1]{0,1,2:T(4,128)S(1)} %copy.293) | copy-start | bytes 772
  71.0 7.0 %copy-start.12 = (f32[16,4,8]{2,1,0:T(4,128)S(1)}, f32[16,4,8]{2,1,0:T(4,128)}, u32[]{:S(2)}) copy-start(f32[16,4,8]{2,1,0:T(4,128)} %copy-done.11) | copy-start | bytes 6148
  81.5 41.9 %reduce-scatter.11.cloned.1.call-start = ((), (), s32[]{:S(2)}) async-start(), calls=%async_computation.5 | async-start | bytes 655360 | tf_op jit(solution)/shard_map/reduce_scatter | solution.py:173
  101.5 44.3 %copy-start.41 = (f32[1,512]{1,0:T(1,128)S(1)}, f32[1,512]{1,0:T(1,128)}, u32[]{:S(2)}) copy-start(f32[1,512]{1,0:T(1,128)} %get-tuple-element.64) | copy-start | bytes 6148
  101.5 80.9 %reduce-scatter.17.cloned.1.call-start = ((), (), s32[]{:S(2)}) async-start(), calls=%async_computation.9 | async-start | bytes 2621440
  152.8 84.8 %all-gather.7.cloned.1.call-start = ((), (), s32[]{:S(2)}) async-start(), calls=%async_computation.6 | async-start | bytes 1310720 | tf_op jit(solution)/shard_map/all_gather | solution.py:168
  182.4 3.2 %copy-start.19 = (f32[1,1,1024]{2,1,0:T(1,128)S(1)}, f32[1,1,1024]{2,1,0:T(1,128)}, u32[]{:S(2)}) copy-start(f32[1,1,1024]{2,1,0:T(1,128)} %get-tuple-element.48) | copy-start | bytes 12292
  185.9 4.6 %copy-start.34 = (bf16[4,768,1,1]{1,0,2,3:T(4,128)(2,1)S(1)}, bf16[4,768,1,1]{1,0,2,3:T(4,128)(2,1)}, u32[]{:S(2)}) copy-start(bf16[4,768,1,1]{1,0,2,3:T(4,128)(2,1)} %get-tuple-element.53) | copy-start | bytes 18436
  187.5 4.8 %copy-start.1 = (bf16[4,16,8,256]{3,2,1,0:T(8,128)(2,1)}, bf16[4,16,8,256]{3,2,1,0:T(8,128)(2,1)S(1)}, u32[]{:S(2)}) copy-start(bf16[4,16,8,256]{3,2,1,0:T(8,128)(2,1)S(1)} %convolution_convert_fusion.8) | copy-start | bytes 786436
  189.0 5.2 %copy-start.4 = (bf16[4,16,8,256]{3,2,1,0:T(8,128)(2,1)}, bf16[4,16,8,256]{3,2,1,0:T(8,128)(2,1)S(1)}, u32[]{:S(2)}) copy-start(bf16[4,16,8,256]{3,2,1,0:T(8,128)(2,1)S(1)} %convolution_convert_fusion.7) | copy-start | bytes 786436
  189.0 3.4 %copy-start.35 = (bf16[4,768,1,1]{1,0,2,3:T(4,128)(2,1)S(1)}, bf16[4,768,1,1]{1,0,2,3:T(4,128)(2,1)}, u32[]{:S(2)}) copy-start(bf16[4,768,1,1]{1,0,2,3:T(4,128)(2,1)} %get-tuple-element.51) | copy-start | bytes 18436
  190.5 3.7 %copy-start.8 = (bf16[4,16,8,256]{3,2,1,0:T(8,128)(2,1)}, bf16[4,16,8,256]{3,2,1,0:T(8,128)(2,1)S(1)}, u32[]{:S(2)}) copy-start(bf16[4,16,8,256]{3,2,1,0:T(8,128)(2,1)S(1)} %convolution_convert_fusion.6) | copy-start | bytes 786436
  190.5 3.7 %copy-start.40 = (f32[4]{0:T(128)S(1)}, f32[4]{0:T(128)}, u32[]{:S(2)}) copy-start(f32[4]{0:T(128)} %get-tuple-element.67) | copy-start | bytes 52
  190.5 6.7 %copy-start.36 = (f32[4]{0:T(128)S(1)}, f32[4]{0:T(128)}, u32[]{:S(2)}) copy-start(f32[4]{0:T(128)} %get-tuple-element.69) | copy-start | bytes 52
  190.5 6.7 %copy-start.39 = (pred[8,8]{1,0:T(8,128)(4,1)S(1)}, pred[8,8]{1,0:T(8,128)(4,1)}, u32[]{:S(2)}) copy-start(pred[8,8]{1,0:T(8,128)(4,1)} %copy-done.38) | copy-start | bytes 196
  204.9 4.1 %copy-start.15 = (f32[16,4,1]{0,1,2:T(4,128)S(1)}, f32[16,4,1]{0,1,2:T(4,128)}, u32[]{:S(2)}) copy-start(f32[16,4,1]{0,1,2:T(4,128)} %copy-done.14) | copy-start | bytes 772
  204.9 4.1 %copy-start.24 = (f32[2,16,4]{1,2,0:T(4,128)S(1)}, f32[2,16,4]{1,2,0:T(4,128)}, u32[]{:S(2)}) copy-start(f32[2,16,4]{1,2,0:T(4,128)} %param.39) | copy-start | bytes 1540
  206.1 5.0 %copy-start.2 = (bf16[4,16,8,256]{3,2,1,0:T(8,128)(2,1)S(1)}, bf16[4,16,8,256]{3,2,1,0:T(8,128)(2,1)}, u32[]{:S(2)}) copy-start(bf16[4,16,8,256]{3,2,1,0:T(8,128)(2,1)} %copy-done.1) | copy-start | bytes 786436
  215.0 48.7 %reduce-scatter.13.cloned.1.call-start = ((), (), s32[]{:S(2)}) async-start(), calls=%async_computation.7 | async-start | bytes 655360 | tf_op jit(solution)/shard_map/reduce_scatter | solution.py:173
  215.9 10.9 %copy-start.7 = (bf16[4,16,8,256]{3,2,1,0:T(8,128)(2,1)S(1)}, bf16[4,16,8,256]{3,2,1,0:T(8,128)(2,1)}, u32[]{:S(2)}) copy-start(bf16[4,16,8,256]{3,2,1,0:T(8,128)(2,1)} %copy-done.6) | copy-start | bytes 786436
  (22 other events, 41.2 us)
Sparse Core Ops, SparseCore 0:
  22.4 32.8 reduce-scatter.14
  81.7 16.6 all-gather.4
  101.6 21.8 reduce-scatter.10
  152.9 29.4 reduce-scatter.16
  215.1 16.7 all-gather.6
  240.8 22.0 reduce-scatter.12
